TPU v7x, 32 devices: a whole 2x2x4 slice. The times are simulated.
32 devices in a mesh: sp: 4 (over z), fs: 4 (over y, x), tp: 2 (over core).
Axes of the slice: x: 2, y: 2, z: 4, core: 2. Of those that a mesh axis runs over, the one named last changes fastest.
Arguments:
- tokens: bfloat16 [4, 1024, 2048], P('fs', 'sp', 'tp'), may hold values from -6 to 6
- norm_gain: float32 [2048], replicated, may hold values from 0.1 to 1.9
- ret_query: bfloat16 [2048, 1024], P('sp', 'tp'), may hold values from -0.125 to 0.125
- ret_key: bfloat16 [2048, 1024], P('sp', 'tp'), may hold values from -0.125 to 0.125
- ret_value: bfloat16 [2048, 1024], P('sp', 'tp'), may hold values from -0.125 to 0.125
- att_query: bfloat16 [2048, 1024], P('sp', 'tp'), may hold values from -0.125 to 0.125
- att_key: bfloat16 [2048, 256], P('sp', 'tp'), may hold values from -0.125 to 0.125
- att_value: bfloat16 [2048, 256], P('sp', 'tp'), may hold values from -0.125 to 0.125
- log_decay: float32 [4, 4, 1024], P('fs', 'tp', 'sp'), may hold values from -1 to 0
- start_state: float32 [4, 4, 256, 256], P('fs', 'tp'), may hold values from -12 to 12
- ret_gain: float32 [1024], P('tp'), may hold values from 0.1 to 1.9
- sink_logits: float32 [16], P('tp'), may hold values from 1 to 5
- ret_out: bfloat16 [1024, 2048], P('tp', 'fs'), may hold values from -0.1875 to 0.1875
- att_out: bfloat16 [1024, 2048], P('tp', 'fs'), may hold values from -1.5 to 1.5
Outputs:
- mixed: bfloat16 [4, 1024, 2048], P('fs', 'sp', 'tp')
All inputs are finite; a program needn't handle non-finite values.
Results may differ from a plain program's by a relative error of at most 0.015.
Values may be sent and summed in bfloat16 or wider, within the bound.
A program may use at most 128 MiB of HBM per device.

v0:
```python
import jax
import jax.numpy as jnp
from jax import lax
from jax.sharding import PartitionSpec as P

DK = 256
DV = 256
HD = 64
WINDOW = 128
BLOCK = 128


epsilon = 1e-06
exact_result = lax.Precision.HIGHEST


def carried_in(array, axis, combine, identity):
    peers, mine = (lax.axis_size(axis), lax.axis_index(axis))
    everything = jax.tree.map(
        lambda part, kind: lax.all_gather(part.astype(kind), axis),
        array,
        (jnp.bfloat16, jnp.bfloat16),
    )
    start = jax.tree.map(
        lambda part, zero: jnp.broadcast_to(jnp.asarray(zero, part.dtype), part.shape),
        array,
        identity,
    )

    def hop(k, before):
        reached = k < mine
        new = combine(
            before, jax.tree.map(lambda part, own: part[k].astype(own.dtype), everything, array)
        )
        return jax.tree.map(lambda a, b: jnp.where(reached, a, b), new, before)

    return lax.fori_loop(0, peers, hop, start)


def passed_along(block, axis, distance):
    devices = range(lax.axis_size(axis))
    route = [(i - distance, i) for i in devices if i - distance in devices]
    return lax.ppermute(block, axis, route)


def rotate(values, positions):
    half_dim = values.shape[-1] // 2
    inverse = 1.0 / 10000.0 ** (jnp.arange(half_dim, dtype=jnp.float32) / half_dim)
    angles = positions.astype(jnp.float32)[:, None] * inverse[None, :]
    cosine = jnp.cos(angles)[:, None, :]
    sine_table = jnp.sin(angles)[:, None, :]
    front_half = values[..., :half_dim]
    back_half = values[..., half_dim:]
    return jnp.concatenate(
        [
            front_half * cosine - back_half * sine_table,
            front_half * sine_table + back_half * cosine,
        ],
        axis=-1,
    )


def block_step(memory_state, inputs):
    queries, key_matrix_rows, value_matrix_rows, log_rates = inputs
    length_here = log_rates.shape[-1]
    causal = jnp.arange(length_here)[:, None] >= jnp.arange(length_here)[None, :]
    running_totals = jnp.cumsum(log_rates, axis=-1)
    relative = running_totals[:, :, None] - running_totals[:, None, :]
    weight = jnp.where(causal[None], jnp.exp(jnp.where(causal[None], relative, 0.0)), 0.0)
    score_matrix = (
        jnp.einsum("hqd,hkd->hqk", queries, key_matrix_rows, precision=exact_result) * weight
    )
    carried_state = jnp.einsum(
        "hqd,hdv->hqv",
        queries * jnp.exp(running_totals)[:, :, None],
        memory_state,
        precision=exact_result,
    )
    output_rows = (
        jnp.einsum("arf,afu->aru", score_matrix, value_matrix_rows, precision=exact_result)
        + carried_state
    )
    decay_factors = jnp.exp(running_totals[:, -1:] - running_totals)
    memory_state = memory_state * jnp.exp(running_totals[:, -1])[:, None, None] + jnp.einsum(
        "iwj,iwe->ije",
        key_matrix_rows * decay_factors[:, :, None],
        value_matrix_rows,
        precision=exact_result,
    )
    return (memory_state, output_rows)


def chain(earlier, later):
    return (earlier[0] * later[0], earlier[1] * later[0][:, None, None] + later[1])


def shards(
    tokens,
    norm_gain,
    ret_query,
    ret_key,
    ret_value,
    att_query,
    att_key,
    att_value,
    log_decay,
    start_state,
    ret_gain,
    sink_logits,
    ret_out,
    att_out,
):
    gathered = lax.all_gather(tokens[0], "tp", axis=1, tiled=True)
    row_count = gathered.shape[0]
    as_float = gathered.astype(jnp.float32)
    normed = (
        as_float
        * lax.rsqrt(jnp.mean(as_float * as_float, axis=-1, keepdims=True) + epsilon)
        * norm_gain
    ).astype(jnp.bfloat16)
    offset = lax.axis_index("sp") * row_count
    positions = offset + jnp.arange(row_count, dtype=jnp.int32)
    weights = (ret_query, ret_key, ret_value, att_query, att_key, att_value)
    pieces = (
        lax.all_gather(weights[0], "sp", axis=0, tiled=True),
        lax.all_gather(weights[1], "sp", axis=0, tiled=True),
        lax.all_gather(weights[2], "sp", axis=0, tiled=True),
        lax.all_gather(weights[3], "sp", axis=0, tiled=True),
        lax.all_gather(weights[4], "sp", axis=0, tiled=True),
        lax.all_gather(weights[5], "sp", axis=0, tiled=True),
    )
    projected = tuple(
        (jnp.dot(normed, piece, preferred_element_type=jnp.float32) for piece in pieces)
    )
    rounded = tuple((product_f.astype(jnp.bfloat16) for product_f in projected))
    projected = rounded[:3]
    head_count = projected[0].shape[1] // DK
    queries = rotate(projected[0].astype(jnp.float32).reshape(row_count, head_count, DK), positions)
    keys_rot = rotate(
        projected[1].astype(jnp.float32).reshape(row_count, head_count, DK), positions
    ) * DK ** (-0.5)
    values_f = projected[2].astype(jnp.float32).reshape(row_count, head_count, DV)
    log_rates = log_decay[0]
    count = row_count // BLOCK

    def blocked(array):
        return array.reshape(count, BLOCK, head_count, array.shape[-1]).transpose(0, 2, 1, 3)

    rates_blocked = log_rates.reshape(head_count, count, BLOCK).transpose(1, 0, 2)
    local_state, pieces = lax.scan(
        block_step,
        jnp.zeros((head_count, DK, DV), jnp.float32),
        (blocked(queries), blocked(keys_rot), blocked(values_f), rates_blocked),
    )
    local_out = pieces.transpose(0, 2, 1, 3).reshape(row_count, head_count, DV)
    running_totals = jnp.cumsum(log_rates, axis=-1)
    device_decay = jnp.exp(running_totals[:, -1])
    identity = (jnp.ones((head_count,), jnp.float32), jnp.zeros((head_count, DK, DV), jnp.float32))
    prior_decay, prior_state = carried_in((device_decay, local_state), "sp", chain, identity)
    incoming = prior_state + prior_decay[:, None, None] * start_state[0]
    retained = local_out + jnp.einsum(
        "thd,hdv->thv",
        queries * jnp.exp(running_totals).T[:, :, None],
        incoming,
        precision=exact_result,
    )
    centred = retained - jnp.mean(retained, axis=-1, keepdims=True)
    variance = jnp.mean(centred * centred, axis=-1, keepdims=True)
    ret_hidden = (
        (centred * lax.rsqrt(variance + epsilon)).reshape(row_count, head_count * DV) * ret_gain
    ).astype(jnp.bfloat16)
    att_queries, att_keys, att_values = rounded[3:]
    kv_heads = att_keys.shape[1] // HD
    groups = att_queries.shape[1] // HD // kv_heads
    earlier_keys, earlier_values = passed_along(
        (att_keys[row_count - WINDOW :], att_values[row_count - WINDOW :]), "sp", 1
    )
    extended_keys = jnp.concatenate([earlier_keys, att_keys], axis=0)
    extended_values = jnp.concatenate([earlier_values, att_values], axis=0)
    windows = row_count // WINDOW

    def banded(array):
        earlier = array[:row_count].reshape(windows, WINDOW, kv_heads, HD)
        current = array[WINDOW:].reshape(windows, WINDOW, kv_heads, HD)
        return jnp.concatenate([earlier, current], axis=1)

    key_band = banded(extended_keys)
    value_band = banded(extended_values)
    grouped_q = att_queries.reshape(windows, WINDOW, kv_heads, groups, HD)
    score_matrix = jnp.einsum(
        "nqhgd,nkhd->nhgqk", grouped_q, key_band, preferred_element_type=jnp.float32
    ) * HD ** (-0.5)
    query_index = WINDOW + jnp.arange(WINDOW)
    key_index = jnp.arange(2 * WINDOW)
    allowed = (key_index[None, :] <= query_index[:, None]) & (
        query_index[:, None] - key_index[None, :] < WINDOW
    )
    key_place = offset - WINDOW + jnp.arange(windows)[:, None] * WINDOW + key_index[None, :]
    visible = (allowed[None] & (key_place >= 0)[:, None, :])[:, None, None]
    expo = jnp.exp(jnp.where(visible, score_matrix, -1e30))
    summed = jnp.sum(expo, axis=-1, keepdims=True) + jnp.exp(sink_logits).reshape(
        1, kv_heads, groups, 1, 1
    )
    probs = (expo / summed).astype(jnp.bfloat16)
    attended = jnp.einsum(
        "nhgqk,nkhd->nqhgd", probs, value_band, preferred_element_type=jnp.float32
    )
    att_hidden = attended.astype(jnp.bfloat16).reshape(row_count, kv_heads * groups * HD)
    ret_width = ret_hidden.shape[1]
    joined = jnp.concatenate([ret_hidden, att_hidden], axis=1)[None]
    piece = lax.all_gather(joined, "fs", axis=0, tiled=True)
    product = jnp.einsum(
        "srh,hd->srd", piece[:, :, :ret_width], ret_out, preferred_element_type=jnp.float32
    )
    product = product + jnp.einsum(
        "srh,hd->srd", piece[:, :, ret_width:], att_out, preferred_element_type=jnp.float32
    )
    partial_rows = product.astype(jnp.bfloat16)
    regrouped = lax.all_to_all(partial_rows, "fs", split_axis=0, concat_axis=2, tiled=True)
    mixed = lax.psum_scatter(
        regrouped[0].astype(jnp.float32).astype(jnp.bfloat16), "tp", scatter_dimension=1, tiled=True
    )
    return mixed[None]


def solution(mesh):
    placed = (
        P("fs", "sp", "tp"),
        P(),
        P("sp", "tp"),
        P("sp", "tp"),
        P("sp", "tp"),
        P("sp", "tp"),
        P("sp", "tp"),
        P("sp", "tp"),
        P("fs", "tp", "sp"),
        P("fs", "tp", None, None),
        P("tp"),
        P("tp"),
        P("tp", "fs"),
        P("tp", "fs"),
    )
    return jax.shard_map(
        shards, mesh=mesh, in_specs=placed, out_specs=P("fs", "sp", "tp"), check_vma=False
    )
```

profile of v0, /device:TPU:0, one launch (start us, length us, event | category | flops | bytes accessed | tf_op | source)
XLA Modules:
  0.0 330.0 jit_solution(6295431087866726067)
XLA Ops:
  13.0 13.6 %all-reduce = bf16[8]{0:T(256)(128)(2,1)S(1)} all-reduce(bf16[8]{0:T(256)(128)(2,1)S(1)} %dynamic-update-slice), channel_id=3, replica_groups=mesh['sp'=4,'fs'=4,'tp'=2] {'sp'}, use_global_device_ids=true, to_apply=%add | all-reduce | flops 8 | bytes 32
  26.6 18.4 %all_gather.42 = bf16[2048,128]{1,0:T(8,128)(2,1)S(1)} all-gather(bf16[512,128]{1,0:T(8,128)(2,1)S(1)} %copy-done.12), channel_id=1, replica_groups=mesh['sp'=4,'fs'=4,'tp'=2] {'sp'}, dimensions={0}, use_global_device_ids=true | all-gather | bytes 655360 | tf_op jit(solution)/shard_map/all_gather | solution.py:129
  45.7 21.2 %all_gather.41 = bf16[2048,128]{1,0:T(8,128)(2,1)} all-gather(bf16[512,128]{1,0:T(8,128)(2,1)S(1)} %copy-done.13), channel_id=1, replica_groups=mesh['sp'=4,'fs'=4,'tp'=2] {'sp'}, dimensions={0}, use_global_device_ids=true | all-gather | bytes 655360 | tf_op jit(solution)/shard_map/all_gather | solution.py:130
  68.9 1.6 fusion.25
  70.5 1.7 convolution_convert_fusion.5
  72.9 2.6 collective-permute-start.1
  75.5 5.5 %all-gather.12.cloned.1.call-done = bf16[2048,512]{1,0:T(8,128)(2,1)} async-done(((bf16[512,512]{1,0:T(8,128)(2,1)}), bf16[2048,512]{1,0:T(8,128)(2,1)}) %all-gather.12.cloned.1.call-update) | async-done | bytes 2097168 | tf_op jit(solution)/shard_map/all_gather | solution.py:126
  80.9 2.3 fusion.31
  83.6 44.0 %all-gather.16.cloned.1.call-done = bf16[2048,512]{1,0:T(8,128)(2,1)} async-done(((bf16[512,512]{1,0:T(8,128)(2,1)}), bf16[2048,512]{1,0:T(8,128)(2,1)}) %all-gather.16.cloned.1.call-update) | async-done | bytes 2097168 | tf_op jit(solution)/shard_map/all_gather | solution.py:125
  127.6 2.7 fusion.33
  131.4 42.1 %all-gather.14.cloned.1.call-done = bf16[2048,512]{1,0:T(8,128)(2,1)} async-done(((bf16[512,512]{1,0:T(8,128)(2,1)}), bf16[2048,512]{1,0:T(8,128)(2,1)}) %all-gather.14.cloned.1.call-update) | async-done | bytes 2097168 | tf_op jit(solution)/shard_map/all_gather | solution.py:127
  173.6 2.7 fusion.32
  178.9 6.7 %while.29 = (s32[]{:T(128)}, f32[2,256,256]{2,1,0:T(8,128)S(1)}, f32[2,2,128,256]{3,2,1,0:T(8,128)}, f32[2,2,128]{2,1,0:T(2,128)S(1)}, f32[2,2,128,256]{3,2,0,1:...) while((s32[]{:T(128)}, f32[2,256,256]{2,1,0:T(8,128)S(1)}, ...), condition=%wide.region_3.4_spmd.clone, body=%wide.region_1.3_spmd.clone.sunk | while | flops 604880896 | bytes 4242084 | solution.py:150
  186.4 1.9 convolution_convert_fusion.6
  188.6 2.3 collective-permute-start
  194.9 24.5 %all-gather.18.cloned.1.call-done = bf16[2048,512]{1,0:T(8,128)(2,1)} async-done(((bf16[512,512]{1,0:T(8,128)(2,1)}), bf16[2048,512]{1,0:T(8,128)(2,1)}) %all-gather.18.cloned.1.call-update) | async-done | bytes 2097168 | tf_op jit(solution)/shard_map/all_gather | solution.py:128
  219.5 2.3 convolution_convert_fusion.1
  223.8 25.1 %all-gather.22.cloned.1.call-done = bf16[8,256,256]{2,1,0:T(8,128)(2,1)} async-done(((bf16[2,256,256]{2,1,0:T(8,128)(2,1)}), bf16[8,256,256]{2,1,0:T(8,128)(2,1)}) %all-gather.22.cloned.1.call-update) | async-done | bytes 1048592 | tf_op jit(solution)/shard_map/all_gather | solution.py:20
  248.9 4.6 %while.30 = (s32[]{:T(128)}, f32[2]{0:T(128)S(1)}, f32[2,256,256]{2,1,0:T(8,128)S(1)}, s32[]{:T(128)}, bf16[4,2]{1,0:T(4,128)(2,1)S(1)}, /*index=5*/bf16[4,2,256,256]{3,2,1,0:T(8,128)(2,1)}, s32[]{:T(128)}, s32[]{:T(128)}) while((s32[]{:T(128)}, f32[2]{0:T(128)S(1)}, f32[2,256,256]{2,1,0:T(8,128)S(1)}, s32[]{:T(128)}, ...), condition=%wide.region_7.8_spmd.clone, body=%wide.region_6.7_spmd.clone.sunk | while | flops 655372 | bytes 1310871 | solution.py:37
  255.9 34.5 %all-gather.24.cloned.1.call-done = bf16[1024,1024]{0,1:T(8,128)(2,1)} async-done(((bf16[256,1024]{0,1:T(8,128)(2,1)}), bf16[1024,1024]{0,1:T(8,128)(2,1)}) %all-gather.24.cloned.1.call-update) | async-done | bytes 2097168 | tf_op jit(solution)/shard_map/all_gather | solution.py:211
  290.4 2.9 copy.81
  295.1 16.7 %all_to_all.15 = bf16[4,256,512]{2,1,0:T(8,128)(2,1)S(1)} all-to-all(bf16[4,256,512]{2,1,0:T(8,128)(2,1)S(1)} %add_convert_fusion), channel_id=1, replica_groups=mesh['sp'=4,'fs'=4,'tp'=2] {'fs'}, dimensions={0} | all-to-all | bytes 2097152 | tf_op jit(solution)/shard_map/all_to_all | solution.py:219
  313.1 8.0 %reduce-scatter.2.cloned.1.call-done = bf16[256,1024]{0,1:T(8,128)(2,1)} async-done(((bf16[256,2048]{0,1:T(8,128)(2,1)}), bf16[256,1024]{0,1:T(8,128)(2,1)}) %reduce-scatter.2.cloned.1.call-update) | async-done | bytes 524304 | tf_op jit(solution)/shard_map/reduce_scatter | solution.py:220
  321.1 2.0 copy.83
  (162 shorter events, 36.5 us)
Async XLA Ops:
  6.5 286.8 %copy-start = (bf16[512,512]{1,0:T(8,128)(2,1)S(1)}, bf16[512,512]{1,0:T(8,128)(2,1)}, u32[]{:S(2)}) copy-start(bf16[512,512]{1,0:T(8,128)(2,1)} %param.30) | copy-start | bytes 1572868
  6.5 4.8 %copy-start.23 = (u32[32]{0:T(128)S(1)}, u32[32]{0:T(128)}, u32[]{:S(2)}) copy-start(u32[32]{0:T(128)} %constant.93) | copy-start | bytes 388
  6.5 20.1 %copy-start.12 = (bf16[512,128]{1,0:T(8,128)(2,1)S(1)}, bf16[512,128]{1,0:T(8,128)(2,1)}, u32[]{:S(2)}) copy-start(bf16[512,128]{1,0:T(8,128)(2,1)} %param.24) | copy-start | bytes 393220
  6.5 38.6 %copy-start.22 = (f32[8]{0:T(128)S(1)}, f32[8]{0:T(128)}, u32[]{:S(2)}) copy-start(f32[8]{0:T(128)} %param.29) | copy-start | bytes 100
  6.5 39.2 %copy-start.13 = (bf16[512,128]{1,0:T(8,128)(2,1)S(1)}, bf16[512,128]{1,0:T(8,128)(2,1)}, u32[]{:S(2)}) copy-start(bf16[512,128]{1,0:T(8,128)(2,1)} %param.25) | copy-start | bytes 393220
  6.6 62.3 %all-gather.20.cloned.1.call-start = ((), (), s32[]{:S(2)}) async-start(), calls=%async_computation.7 | async-start | bytes 1572864 | tf_op jit(solution)/shard_map/all_gather | solution.py:113
  7.3 73.6 %all-gather.12.cloned.1.call-start = ((), (), s32[]{:S(2)}) async-start(), calls=%async_computation.2 | async-start | bytes 2621440 | tf_op jit(solution)/shard_map/all_gather | solution.py:126
  8.0 62.5 %copy-start.20 = (f32[2048]{0:T(1024)S(1)}, f32[2048]{0:T(1024)}, u32[]{:S(2)}) copy-start(f32[2048]{0:T(1024)} %param.19) | copy-start | bytes 24580
  8.1 119.6 %all-gather.16.cloned.1.call-start = ((), (), s32[]{:S(2)}) async-start(), calls=%async_computation.4 | async-start | bytes 2621440 | tf_op jit(solution)/shard_map/all_gather | solution.py:125
  8.8 164.8 %all-gather.14.cloned.1.call-start = ((), (), s32[]{:S(2)}) async-start(), calls=%async_computation.3 | async-start | bytes 2621440 | tf_op jit(solution)/shard_map/all_gather | solution.py:127
  9.4 210.1 %all-gather.18.cloned.1.call-start = ((), (), s32[]{:S(2)}) async-start(), calls=%async_computation.5 | async-start | bytes 2621440 | tf_op jit(solution)/shard_map/all_gather | solution.py:128
  10.0 238.9 %all-gather.22.cloned.1.call-start = ((), (), s32[]{:S(2)}) async-start(), calls=%async_computation.8 | async-start | bytes 1310720 | tf_op jit(solution)/shard_map/all_gather | solution.py:20
  68.9 12.1 %copy-start.5 = (bf16[1,256,2048]{2,1,0:T(8,128)(2,1)S(1)}, bf16[1,256,2048]{2,1,0:T(8,128)(2,1)}, u32[]{:S(2)}) copy-start(bf16[1,256,2048]{2,1,0:T(8,128)(2,1)} %all-gather.20.cloned.1.call-done) | copy-start | bytes 3145732
  70.5 103.1 %copy-start.18 = (f32[256]{0:T(256)}, f32[256]{0:T(256)S(1)}, u32[]{:S(2)}) copy-start(f32[256]{0:T(256)S(1)} %add_rsqrt_fusion.1) | copy-start | bytes 3076
  72.2 11.0 %copy-start.10 = (bf16[256,128]{1,0:T(8,128)(2,1)}, bf16[256,128]{1,0:T(8,128)(2,1)S(1)}, u32[]{:S(2)}) copy-start(bf16[256,128]{1,0:T(8,128)(2,1)S(1)} %convolution_convert_fusion.5) | copy-start | bytes 196612
  72.9 118.2 %collective-permute-start.1 = (bf16[128,128]{1,0:T(8,128)(2,1)}, bf16[128,128]{1,0:T(8,128)(2,1)}, u32[]{:S(2)}, u32[]{:S(2)}) collective-permute-start(bf16[128,128]{1,0:T(8,128)(2,1)} %slice.64), channel_id=1, source_target_pairs={{0,8},{8,16},{16,24},{1,9},{9,17},{17,25},{2,10},{10,18},{18,26},{... | collective-permute-start | bytes 98312 | tf_op jit(solution)/shard_map/ppermute | solution.py:43
  178.8 7.6 %copy-start.19 = (f32[256]{0:T(256)S(1)}, f32[256]{0:T(256)}, u32[]{:S(2)}) copy-start(f32[256]{0:T(256)} %copy-done.18) | copy-start | bytes 3076
  178.8 7.6 %copy-start.21 = (f32[2048]{0:T(1024)S(1)}, f32[2048]{0:T(1024)}, u32[]{:S(2)}) copy-start(f32[2048]{0:T(1024)} %param.19) | copy-start | bytes 24580
  186.4 104.1 %all-gather.24.cloned.1.call-start = ((), (), s32[]{:S(2)}) async-start(), calls=%async_computation.9 | async-start | bytes 2621440 | tf_op jit(solution)/shard_map/all_gather | solution.py:211
  188.3 31.2 %copy-start.6 = (bf16[1,256,2048]{2,1,0:T(8,128)(2,1)S(1)}, bf16[1,256,2048]{2,1,0:T(8,128)(2,1)}, u32[]{:S(2)}) copy-start(bf16[1,256,2048]{2,1,0:T(8,128)(2,1)} %all-gather.20.cloned.1.call-done) | copy-start | bytes 3145732
  188.6 4.3 %collective-permute-start = (bf16[128,128]{1,0:T(8,128)(2,1)S(1)}, bf16[128,128]{1,0:T(8,128)(2,1)S(1)}, u32[]{:S(2)}, u32[]{:S(2)}) collective-permute-start(bf16[128,128]{1,0:T(8,128)(2,1)S(1)} %slice.63), channel_id=1, source_target_pairs={{0,8},{8,16},{16,24},{1,9},{9,17},{17,25},{2,10},{10,18},{18,26},{... | collective-permute-start | bytes 98312 | tf_op jit(solution)/shard_map/ppermute | solution.py:43
  194.9 27.2 %copy-start.14 = (pred[2,128,256]{1,2,0:T(8,128)(4,1)S(1)}, pred[2,128,256]{1,2,0:T(8,128)(4,1)}, u32[]{:S(2)}) copy-start(pred[2,128,256]{1,2,0:T(8,128)(4,1)} %broadcast_and_fusion) | copy-start | bytes 196612
  248.9 4.6 %copy-start.9 = (f32[1,2,256,256]{3,2,1,0:T(8,128)S(1)}, f32[1,2,256,256]{3,2,1,0:T(8,128)}, u32[]{:S(2)}) copy-start(f32[1,2,256,256]{3,2,1,0:T(8,128)} %param.27) | copy-start | bytes 1572868
  255.9 65.2 %reduce-scatter.2.cloned.1.call-start = ((), (), s32[]{:S(2)}) async-start(), calls=%async_computation.6 | async-start | bytes 1572864 | tf_op jit(solution)/shard_map/reduce_scatter | solution.py:220
  (10 other events, 21.6 us)
Sparse Core Ops, SparseCore 0:
  8.9 11.7 all-gather.19
  22.3 58.6 all-gather.11
  82.5 45.0 all-gather.15
  129.1 44.4 all-gather.13
  175.0 44.4 all-gather.17
  220.9 27.9 all-gather.21
  256.0 34.4 all-gather.23
  313.2 7.8 reduce-scatter.1
where the time goes:
time: 331 us; the launch traced here: 330 us
  waiting for transfers between devices  188 us (57%)
  blocking collectives  69.8 us (21%)
  matrix products  23 us (7%)
  local copies, waits for them, and re-layouts  16.4 us (5%)
  between operations  14.8 us (4%)
  other arithmetic  12.8 us (4%)
  starting transfers between devices  5.19 us (2%)
    all_gather x1, waiting for transfers between devices, shards(): lax.all_gather(weights[0], 'sp', axis=0, tiled=True)  44 us
    all_gather x1, waiting for transfers between devices, shards(): lax.all_gather(weights[2], 'sp', axis=0, tiled=True)  42.1 us
    all_gather x1, waiting for transfers between devices, shards(): piece = lax.all_gather(joined, 'fs', axis=0, tiled=True)  34.5 us
    all_gather x1, waiting for transfers between devices, carried_in(): lax.all_gather(part.astype(kind), axis)  25.1 us
    all_gather x1, waiting for transfers between devices, shards(): lax.all_gather(weights[3], 'sp', axis=0, tiled=True)  24.5 us
    all_gather x1, blocking collectives, shards(): lax.all_gather(weights[5], 'sp', axis=0, tiled=True)  21.2 us
    all_gather x1, blocking collectives, shards(): lax.all_gather(weights[4], 'sp', axis=0, tiled=True)  18.4 us
    all_to_all x1, blocking collectives, shards(): lax.all_to_all(partial_rows, 'fs', split_axis=0, concat_axis=2, tiled=True)  16.7 us
  transfers between devices with their start and end apart: 10, of which 8 were waited for; matrix products, arithmetic and copies ran while one was open for 11% of the time, Pallas kernels for 0%

commit v1 on v0

--- a/solution.py
+++ b/solution.py
@@ -1,6 +1,11 @@
+import functools
+
 import jax
 import jax.numpy as jnp
+import numpy as np
 from jax import lax
+from jax.experimental import pallas as pl
+from jax.experimental.pallas import tpu as pltpu
 from jax.sharding import PartitionSpec as P
 
 DK = 256
@@ -223,6 +228,420 @@
     return mixed[None]
 
 
+MESH = pl.DeviceIdType.MESH
+F32 = jnp.float32
+BF16 = jnp.bfloat16
+GAIN_ROW = 0
+DECAY_ROW = 1
+SINK_ROW = 8
+
+
+def dot(a, b):
+    return jnp.dot(a, b, preferred_element_type=F32)
+
+
+def dot_t(a, b):
+    return lax.dot_general(a, b, (((1,), (1,)), ((), ())), preferred_element_type=F32)
+
+
+def dot_l(a, b):
+    return lax.dot_general(a, b, (((0,), (0,)), ((), ())), preferred_element_type=F32)
+
+
+def fused(
+    n_sp, n_fs, tok, ngain, rq, rk, rv, aq, ak, av, small, start, ro, ao, cos, sin, out,
+    toks, ss_mine, ss_peer, w, wo, sm, s0, proj, kv, hid, hin, state,
+    send, wsem, wpsem, smsem, ssem, sssem, tsem, osem, hsem, lsem,
+):
+    z, f, c = lax.axis_index("sp"), lax.axis_index("fs"), lax.axis_index("tp")
+    peer = 1 - c
+    rows, half = tok.shape
+    depth = rq.shape[0]
+    quarter = depth // n_fs
+    heads_core = rq.shape[1] // DK
+    kvw = ak.shape[1]
+    groups = aq.shape[1] // kvw
+    qw = groups * HD
+    ret_cols, att_cols = 3 * DK, qw + 2 * kvw
+    sub = lax.rem(z, heads_core)
+    is0, is1 = c == 0, c == 1
+
+    barrier = pltpu.get_barrier_semaphore()
+    count = 0
+
+    def greet(**where):
+        pl.semaphore_signal(barrier, inc=1, device_id=where, device_id_type=MESH)
+
+    greet(tp=peer)
+    for t in range(2):
+        for i in range(1, n_sp):
+            greet(sp=lax.rem(z + i, n_sp), tp=jnp.int32(t))
+            count += 1
+        for i in range(1, n_fs):
+            greet(fs=lax.rem(f + i, n_fs), tp=jnp.int32(t))
+            count += 1
+    pl.semaphore_wait(barrier, count + 1)
+
+    sent = []
+    slots = iter(range(send.shape[0]))
+
+    def both(a, b):
+        if a is None:
+            return b
+        return a if b is None else jnp.logical_and(a, b)
+
+    def remote(cond, src, dst, rsem, slot=None, **where):
+        slot = next(slots) if slot is None else slot
+        copy = pltpu.make_async_remote_copy(
+            src_ref=src, dst_ref=dst, send_sem=send.at[slot], recv_sem=rsem,
+            device_id=where, device_id_type=MESH,
+        )
+        sent.append((cond, copy))
+        if cond is None:
+            copy.start()
+        else:
+            pl.when(cond)(copy.start)
+
+    def local(cond, src, dst, sem):
+        pl.when(cond)(pltpu.make_async_copy(src, dst, sem).start)
+
+    def arrived(dst, sem):
+        pltpu.make_async_copy(dst, dst, sem).wait()
+
+    def wrows(at, n):
+        return pl.ds(pl.multiple_of(at, quarter), n)
+
+    def pieces(j, kind):
+        if kind == 0:
+            return [(a, pl.ds(j * DK, DK), pl.ds(i * DK, DK)) for i, a in enumerate((rq, rk, rv))]
+        return [
+            (aq, pl.ds(j * qw, qw), pl.ds(0, qw)),
+            (ak, pl.ds(0, kvw), pl.ds(qw, kvw)),
+            (av, pl.ds(0, kvw), pl.ds(qw + kvw, kvw)),
+        ]
+
+    mine = pl.ds(pl.multiple_of(f * quarter, quarter), quarter)
+    for j in range(heads_core):
+        p = heads_core * c + j
+        away = p != z
+        here = p == z
+        for kind in range(2):
+            remote(away, small, sm.at[z], smsem.at[z], sp=p, tp=jnp.int32(kind))
+            for i, (a, cs, cd) in enumerate(pieces(j, kind)):
+                remote(
+                    away, a.at[mine, cs], w.at[wrows(z * depth + f * quarter, quarter), cd],
+                    wsem.at[z, i], sp=p, tp=jnp.int32(kind),
+                )
+        remote(here, small, sm.at[z], smsem.at[z], tp=peer)
+        local(here, small, sm.at[z], smsem.at[z])
+        for kind in range(2):
+            same, other = both(here, c == kind), both(here, c != kind)
+            for i, (a, cs, cd) in enumerate(pieces(j, kind)):
+                dst = w.at[wrows(z * depth, depth), cd]
+                local(same, a.at[:, cs], dst, wsem.at[z, i])
+                remote(other, a.at[:, cs], dst, wsem.at[z, i], tp=peer)
+        local(both(here, is0), start.at[j], s0, ssem)
+        remote(both(here, is1), start.at[j], s0, ssem, tp=peer)
+
+    x = tok[...].astype(F32)
+    sq = x * x
+    part = sq[:, :128]
+    for i in range(1, half // 128):
+        part = part + sq[:, i * 128 : (i + 1) * 128]
+    ss_mine[...] = part
+    remote(None, ss_mine, ss_peer, sssem, tp=peer)
+    arrived(ss_peer, sssem)
+    mean = jnp.sum(ss_mine[...] + ss_peer[...], axis=-1, keepdims=True) / (2 * half)
+    scale = lax.rsqrt(mean + epsilon)
+    g = ngain[:, pl.ds(pl.multiple_of(c * half, 128), half)]
+    toks[z, c] = (tok[...].astype(F32) * scale * g).astype(BF16)
+
+    def spread(zs, cond, up, down):
+        block = toks.at[zs, c]
+        if up is not None:
+            remote(both(cond, up), block, block, tsem.at[zs, c], sp=lax.rem(z + 1, n_sp))
+        if down is not None:
+            remote(both(cond, down), block, block, tsem.at[zs, c], sp=lax.rem(z + n_sp - 1, n_sp))
+        remote(cond, block, block, tsem.at[zs, c], tp=peer)
+
+    spread(z, None, z < n_sp - 1, z > 0)
+
+    def widths(act):
+        for kind, cols in ((0, ret_cols), (1, att_cols)):
+            act(c == kind, pl.ds(0, cols))
+
+    for i in range(1, n_sp):
+        zs = lax.rem(z + i, n_sp)
+        at = wrows(zs * depth + f * quarter, quarter)
+        for kind in range(2):
+            @pl.when(c == kind)
+            def _():
+                for n, (_, _, cd) in enumerate(pieces(0, kind)):
+                    arrived(w.at[at, cd], wsem.at[zs, n])
+        base = [next(slots) for _ in range(n_fs - 1)]
+        for kind, cols in ((0, ret_cols), (1, att_cols)):
+            for k in range(1, n_fs):
+                block = w.at[at, pl.ds(0, cols)]
+                remote(c == kind, block, block, wpsem.at[zs, f], slot=base[k - 1],
+                       fs=lax.rem(f + k, n_fs))
+
+    fs_core = n_fs // 2
+    owner = f // fs_core
+    jf = lax.rem(f, fs_core)
+    out_rows, out_cols = ro.shape
+    for kind, a in enumerate((ro, ao)):
+        dst = wo.at[kind, pl.ds(pl.multiple_of(c * out_rows, out_rows), out_rows),
+                    pl.ds(pl.multiple_of(jf * out_cols, out_cols), out_cols)]
+        sem = osem.at[kind, c, jf]
+        for k in range(1, n_fs):
+            remote(None, a, dst, sem, fs=lax.rem(f + k, n_fs), tp=owner)
+        local(c == owner, a, dst, sem)
+        remote(c != owner, a, dst, sem, tp=peer)
+
+    for kind, cols in ((0, ret_cols), (1, att_cols)):
+        @pl.when(c == kind)
+        def _():
+            for n, (_, _, cd) in enumerate(pieces(0, kind)):
+                arrived(w.at[wrows(z * depth, depth), cd], wsem.at[z, n])
+            for i in range(1, n_sp):
+                zs = lax.rem(z + i, n_sp)
+                for k in range(1, n_fs):
+                    fs = lax.rem(f + k, n_fs)
+                    arrived(w.at[wrows(zs * depth + fs * quarter, quarter), pl.ds(0, cols)],
+                            wpsem.at[zs, fs])
+    for i in range(n_sp):
+        arrived(sm.at[i], smsem.at[i])
+    kv[pl.ds(0, WINDOW), :] = jnp.zeros((WINDOW, kv.shape[1]), BF16)
+
+    def project(zs):
+        at = pl.ds(pl.multiple_of(zs * rows, rows), rows)
+
+        def tile(cols):
+            return dot(toks[zs, 0], w[pl.ds(0, half), cols]) + dot(toks[zs, 1], w[pl.ds(half, half), cols])
+
+        @pl.when(is0)
+        def _():
+            @pl.loop(0, 3)
+            def _(i):
+                cols = pl.ds(pl.multiple_of(i * DK, DK), DK)
+                proj[at, cols] = tile(cols).astype(BF16)
+
+            co, si = cos[at, :], sin[at, :]
+            h = DK // 2
+            for i, factor in ((0, 1.0), (1, DK ** (-0.5))):
+                a = proj[at, pl.ds(i * DK, h)].astype(F32)
+                b = proj[at, pl.ds(i * DK + h, h)].astype(F32)
+                proj[at, pl.ds(i * DK, h)] = ((a * co - b * si) * factor).astype(BF16)
+                proj[at, pl.ds(i * DK + h, h)] = ((a * si + b * co) * factor).astype(BF16)
+
+        @pl.when(is1)
+        def _():
+            proj[at, pl.ds(0, qw)] = tile(pl.ds(0, qw)).astype(BF16)
+            both_kv = tile(pl.ds(qw, 2 * kvw))
+            to = pl.ds(pl.multiple_of(WINDOW + zs * rows, WINDOW), rows)
+            for n in range(2):
+                got = both_kv[:, n * kvw : n * kvw + HD]
+                for s in range(1, heads_core):
+                    got = jnp.where(sub == s, both_kv[:, n * kvw + s * HD : n * kvw + (s + 1) * HD], got)
+                kv[to, pl.ds(n * 128, HD)] = got.astype(BF16)
+
+    def peer_half(zs):
+        arrived(toks.at[zs, peer], tsem.at[zs, peer])
+
+    def later(zs, cond):
+        def run():
+            peer_half(zs)
+            project(zs)
+        if cond is None:
+            run()
+        else:
+            pl.when(cond)(run)
+
+    waiting = [(z, None)]
+    for d in range(1, n_sp):
+        new = []
+        for s in (-1, 1):
+            zs = z + s * d
+            ok = zs >= 0 if s < 0 else zs < n_sp
+            zs = jnp.clip(zs, 0, n_sp - 1)
+            pl.when(ok)(functools.partial(arrived, toks.at[zs, c], tsem.at[zs, c]))
+            if s < 0:
+                spread(zs, ok, z < n_sp - 1, None)
+            else:
+                spread(zs, ok, None, z > 0)
+            new.append((zs, ok))
+            if waiting:
+                later(*waiting.pop(0))
+        for item in waiting:
+            later(*item)
+        waiting = new
+    for item in waiting:
+        later(*item)
+
+    lane = lax.broadcasted_iota(jnp.int32, (BLOCK, BLOCK), 1)
+    row = lax.broadcasted_iota(jnp.int32, (BLOCK, BLOCK), 0)
+    per = rows // BLOCK
+
+    def retention(p, i):
+        b = p * per + i
+        at = pl.ds(pl.multiple_of(b * BLOCK, BLOCK), BLOCK)
+        l = sm[p, pl.ds(DECAY_ROW, 1), pl.ds(pl.multiple_of(sub * rows + i * BLOCK, BLOCK), BLOCK)]
+        cum = jnp.sum(jnp.where(lane <= row, l, 0.0), axis=1, keepdims=True)
+        cum_row = jnp.sum(jnp.where(lane == row, cum, 0.0), axis=0, keepdims=True)
+        total = jnp.sum(l, axis=1, keepdims=True)
+        weight = jnp.where(lane <= row, jnp.exp(jnp.where(lane <= row, cum - cum_row, 0.0)), 0.0)
+        q, k, v = (proj[at, pl.ds(n * DK, DK)] for n in range(3))
+        st = state[...]
+        scores = (dot_t(q, k) * weight).astype(BF16)
+        o = dot(scores, v) + dot((q.astype(F32) * jnp.exp(cum)).astype(BF16), st.astype(BF16))
+        kd = (k.astype(F32) * jnp.exp(total - cum)).astype(BF16)
+        state[...] = st * jnp.exp(total) + dot_l(kd, v)
+        centred = o - jnp.mean(o, axis=-1, keepdims=True)
+        var = jnp.mean(centred * centred, axis=-1, keepdims=True)
+        gain = sm[z, pl.ds(GAIN_ROW, 1), pl.ds(pl.multiple_of(sub * DV, DV), DV)]
+        hid[at, :] = (centred * lax.rsqrt(var + epsilon) * gain).astype(BF16)
+
+    lane2 = lax.broadcasted_iota(jnp.int32, (WINDOW, 2 * WINDOW), 1)
+    row2 = lax.broadcasted_iota(jnp.int32, (WINDOW, 2 * WINDOW), 0)
+
+    def attention(p, i):
+        b = p * per + i
+        at = pl.ds(pl.multiple_of(b * WINDOW, WINDOW), WINDOW)
+        band = pl.ds(pl.multiple_of(b * WINDOW, WINDOW), 2 * WINDOW)
+        k, v = kv[band, pl.ds(0, HD)], kv[band, pl.ds(128, HD)]
+        visible = (lane2 <= row2 + WINDOW) & (lane2 > row2) & (lane2 + b * WINDOW >= WINDOW)
+        sinks = sm[z, pl.ds(SINK_ROW, heads_core * groups), pl.ds(0, 128)]
+        res = []
+        for h in range(groups):
+            q = proj[at, pl.ds(h * HD, HD)]
+            score = dot_t(q, k) * HD ** (-0.5)
+            e = jnp.exp(jnp.where(visible, score, -1e30))
+            logit = sinks[h : h + 1, :1]
+            for s in range(1, heads_core):
+                logit = jnp.where(sub == s, sinks[s * groups + h : s * groups + h + 1, :1], logit)
+            sink = jnp.exp(logit)
+            total = jnp.sum(e, axis=-1, keepdims=True) + sink
+            res.append(dot((e / total).astype(BF16), v))
+        hid[at, :] = jnp.concatenate(res, axis=1).astype(BF16)
+
+    @pl.when(is0)
+    def _():
+        arrived(s0, ssem)
+        state[...] = s0[...]
+
+    for p in range(n_sp):
+        @pl.when(is0)
+        def _():
+            pl.loop(0, per)(functools.partial(retention, p))
+
+        @pl.when(is1)
+        def _():
+            pl.loop(0, per)(functools.partial(attention, p))
+
+        block = hid.at[pl.ds(p * rows, rows)]
+        remote(z != p, block, hin.at[c, z], hsem.at[c, z], sp=jnp.int32(p))
+        local(z == p, block, hin.at[c, z], hsem.at[c, z])
+
+    for i in range(n_sp):
+        zs = lax.rem(z + i, n_sp)
+        arrived(hin.at[c, zs], hsem.at[c, zs])
+        remote(None, hin.at[c, zs], hin.at[c, zs], hsem.at[c, zs], tp=peer)
+    for kind in range(2):
+        for cs in range(2):
+            for j in range(fs_core):
+                arrived(wo.at[kind, pl.ds(cs * out_rows, out_rows), pl.ds(j * out_cols, out_cols)],
+                        osem.at[kind, cs, j])
+    for zs in range(n_sp):
+        arrived(hin.at[peer, zs], hsem.at[peer, zs])
+
+    @pl.loop(0, out.shape[1] // 256)
+    def _(i):
+        cols = pl.ds(pl.multiple_of(i * 256, 256), 256)
+        acc = None
+        for kind in range(2):
+            for h in range(n_sp):
+                width = hin.shape[3]
+                term = dot(hin[kind, h], wo[kind, pl.ds(h * width, width), cols])
+                acc = term if acc is None else acc + term
+        out[:, cols] = acc.astype(BF16)
+
+    for cond, copy in sent:
+        if cond is None:
+            copy.wait_send()
+        else:
+            pl.when(cond)(copy.wait_send)
+
+
+def layer(mesh, *args):
+    (tokens, norm_gain, ret_query, ret_key, ret_value, att_query, att_key, att_value,
+     log_decay, start_state, ret_gain, sink_logits, ret_out, att_out) = args
+    n_sp, n_fs, n_tp = mesh.shape["sp"], mesh.shape["fs"], mesh.shape["tp"]
+    heads = ret_query.shape[1] // DK
+    kv_heads = att_key.shape[1] // HD
+    rows, half = tokens.shape[1:]
+    whole_heads = (
+        n_tp == 2 and n_fs % 2 == 0 and heads * n_tp == n_sp and kv_heads == heads
+        and att_query.shape[1] == ret_query.shape[1]
+    )
+    if not whole_heads:
+        return shards(*args)
+    depth = ret_query.shape[0]
+    wide = heads * rows
+    decay = log_decay[0].reshape(1, wide)
+    small = jnp.concatenate([
+        jnp.pad(ret_gain[None], ((0, 0), (0, wide - ret_gain.shape[0]))),
+        decay,
+        jnp.zeros((SINK_ROW - 2, wide), F32),
+        jnp.broadcast_to(sink_logits[:, None], (sink_logits.shape[0], wide)),
+    ])
+    h = DK // 2
+    inverse = np.float32(1.0) / np.float32(10000.0) ** (np.arange(h, dtype=np.float32) / np.float32(h))
+    angles = np.arange(n_sp * rows, dtype=np.float32)[:, None] * inverse[None, :]
+    cos = jnp.asarray(np.cos(angles), F32)
+    sin = jnp.asarray(np.sin(angles), F32)
+    length = n_sp * rows
+    vm = pl.BlockSpec(memory_space=pltpu.VMEM)
+    hbm = pl.BlockSpec(memory_space=pl.ANY)
+    dma = pltpu.SemaphoreType.DMA
+    res = pl.pallas_call(
+        functools.partial(fused, n_sp, n_fs),
+        out_shape=jax.ShapeDtypeStruct((rows, half), BF16),
+        in_specs=[vm, vm] + [hbm] * 6 + [vm, hbm, hbm, hbm, vm, vm],
+        out_specs=vm,
+        scratch_shapes=[
+            pltpu.VMEM((n_sp, 2, rows, half), BF16),
+            pltpu.VMEM((rows, 128), F32),
+            pltpu.VMEM((rows, 128), F32),
+            pltpu.VMEM((n_sp * depth, 3 * DK), BF16),
+            pltpu.VMEM((2, 2 * ret_out.shape[0], n_fs // 2 * ret_out.shape[1]), BF16),
+            pltpu.VMEM((n_sp,) + small.shape, F32),
+            pltpu.VMEM((DK, DV), F32),
+            pltpu.VMEM((length, 3 * DK), BF16),
+            pltpu.VMEM((WINDOW + length, 256), BF16),
+            pltpu.VMEM((length, DV), BF16),
+            pltpu.VMEM((2, n_sp, rows, DV), BF16),
+            pltpu.VMEM((DK, DV), F32),
+            dma((100,)),
+            dma((n_sp, 3)),
+            dma((n_sp, n_fs)),
+            dma((n_sp,)),
+            dma,
+            dma,
+            dma((n_sp, 2)),
+            dma((2, 2, n_fs // 2)),
+            dma((2, n_sp)),
+            dma,
+        ],
+        compiler_params=pltpu.CompilerParams(
+            collective_id=0, has_side_effects=True, vmem_limit_bytes=48 * 1024 * 1024
+        ),
+    )(
+        tokens[0], norm_gain[None], ret_query, ret_key, ret_value, att_query, att_key, att_value,
+        small, start_state[0], ret_out, att_out, cos, sin,
+    )
+    return res[None]
+
+
 def solution(mesh):
     placed = (
         P("fs", "sp", "tp"),
@@ -241,5 +660,5 @@
         P("tp", "fs"),
     )
     return jax.shard_map(
-        shards, mesh=mesh, in_specs=placed, out_specs=P("fs", "sp", "tp"), check_vma=False
-    )
+        functools.partial(layer, mesh), mesh=mesh, in_specs=placed, out_specs=P("fs", "sp", "tp"), check_vma=False
+    )

time: 331 us -> 123 us (0.37)
  the two profiles are of different devices: /device:TPU:0 before, /device:TPU:28 now
where the time goes in v1:
time: 123 us; the launch traced here: 122 us
  Pallas kernels  106 us (86%)
  local copies, waits for them, and re-layouts  15.7 us (13%)
    pallas_call x1, Pallas kernels, layer(): pl.pallas_call(functools.partial(fused, n_sp, n_fs), out_shape=jax.ShapeD...  106 us
    unnamed x34, local copies, waits for them, and re-layouts  15.6 us

profile of v1, /device:TPU:28, one launch (start us, length us, event | category | flops | bytes accessed | tf_op | source)
XLA Modules:
  0.0 122.3 jit_solution(10721449612000322902)
XLA Ops:
  0.0 0.7 copy-done.15
  0.7 0.1 pad.3.clone
  0.7 0.1 pad.2.clone
  0.8 0.6 copy-done.14
  1.4 0.0 copy-start.13
  1.4 0.7 copy-done.13
  2.1 0.0 copy-start.12
  2.1 0.1 maximum_maximum_fusion.small
  2.2 0.6 copy-done.12
  2.8 0.0 copy-start
  2.8 1.0 copy-done
  3.8 1.0 copy-done.1
  4.9 1.0 copy-done.2
  5.9 1.0 copy-done.3
  7.0 1.0 copy-done.4
  8.0 1.0 copy-done.5
  9.0 1.0 copy-done.6
  10.1 1.0 copy-done.7
  11.1 1.0 copy-done.8
  12.2 1.0 copy-done.9
  13.2 0.9 copy-done.10
  14.1 0.9 copy-done.11
  15.0 106.5 %shard_map.154 = bf16[256,1024]{1,0:T(8,128)(2,1)S(1)} custom-call(bf16[256,1024]{1,0:T(8,128)(2,1)S(1)} %bitcast.8, f32[1,2048]{1,0:T(1,128)S(1)} %bitcast.10, bf16[512,512]{1,0:T(8,128)(2,1)S(1)} %copy-done.1, bf16[512,512]{1,0:T(8,128)(2,1)S(1)} %copy-done.2, bf16[512,512]{1,0:T(8,128)(2,1)S(1)} %copy-done.3, bf16[512,512]{1,0:T(8,128)(2,1)S(1)} %copy-done.4, ...), custom_call_target="tpu_custom_call" | custom-call | tf_op jit(solution)/shard_map/pallas_call | solution.py:606
  121.5 0.8 copy.19
  (15 shorter events, 0.0 us)
Async XLA Ops:
  0.0 0.7 copy-start.15
  0.7 0.7 copy-start.14
  1.4 0.7 copy-start.13
  2.1 0.7 copy-start.12
  2.8 1.0 copy-start
  3.8 1.0 copy-start.1
  4.9 1.0 copy-start.2
  5.9 1.0 copy-start.3
  7.0 1.0 copy-start.4
  8.0 1.0 copy-start.5
  9.0 1.0 copy-start.6
  10.1 1.0 copy-start.7
  11.1 1.0 copy-start.8
  12.2 1.0 copy-start.9
  13.2 0.9 copy-start.10
  14.1 0.9 copy-start.11

commit v2 on v1

--- a/solution.py
+++ b/solution.py
@@ -249,12 +249,22 @@
 
 
 def fused(
-    n_sp, n_fs, tok, ngain, rq, rk, rv, aq, ak, av, small, start, ro, ao, cos, sin, out,
+    n_sp, n_fs, tok_in, ngain_in, rq, rk, rv, aq, ak, av, gain_in, decay_in, sink_in, start, ro, ao, cos_in, sin_in, out,
+    tok, ngain, small, cos, sin, gain_v, decay_v, sink_v, insem,
     toks, ss_mine, ss_peer, w, wo, sm, s0, proj, kv, hid, hin, state,
     send, wsem, wpsem, smsem, ssem, sssem, tsem, osem, hsem, lsem,
 ):
     z, f, c = lax.axis_index("sp"), lax.axis_index("fs"), lax.axis_index("tp")
     peer = 1 - c
+    inputs = [
+        pltpu.make_async_copy(src, dst, insem.at[i])
+        for i, (src, dst) in enumerate(
+            ((tok_in, tok), (ngain_in, ngain), (gain_in, gain_v), (decay_in, decay_v),
+             (sink_in, sink_v), (cos_in, cos), (sin_in, sin))
+        )
+    ]
+    for copy in inputs:
+        copy.start()
     rows, half = tok.shape
     depth = rq.shape[0]
     quarter = depth // n_fs
@@ -310,6 +320,19 @@
 
     def wrows(at, n):
         return pl.ds(pl.multiple_of(at, quarter), n)
+
+    for copy in inputs[2:5]:
+        copy.wait()
+    small[...] = jnp.zeros_like(small)
+    small[pl.ds(GAIN_ROW, 1), pl.ds(0, gain_v.shape[1])] = gain_v[...]
+    for j in range(heads_core):
+        small[pl.ds(DECAY_ROW, 1), pl.ds(j * rows, rows)] = decay_v[pl.ds(j, 1), :]
+    n_sink = sink_v.shape[1]
+    diagonal = lax.broadcasted_iota(jnp.int32, (n_sink, n_sink), 0) == lax.broadcasted_iota(
+        jnp.int32, (n_sink, n_sink), 1
+    )
+    column = jnp.sum(jnp.where(diagonal, sink_v[...], 0.0), axis=1, keepdims=True)
+    small[pl.ds(SINK_ROW, n_sink), :] = jnp.broadcast_to(column, (n_sink, small.shape[1]))
 
     def pieces(j, kind):
         if kind == 0:
@@ -343,6 +366,38 @@
         local(both(here, is0), start.at[j], s0, ssem)
         remote(both(here, is1), start.at[j], s0, ssem, tp=peer)
 
+    fs_core = n_fs // 2
+    owner = f // fs_core
+    out_rows, out_cols = ro.shape
+
+    def out_block(kind, core, fsrc):
+        j = lax.rem(fsrc, fs_core)
+        block = wo.at[kind, pl.ds(pl.multiple_of(core * out_rows, out_rows), out_rows),
+                      pl.ds(pl.multiple_of(j * out_cols, out_cols), out_cols)]
+        return block, osem.at[kind, core, j]
+
+    beside, across = f + 1 - 2 * lax.rem(f, 2), lax.rem(f + 2, n_fs)
+    corner = lax.rem(beside + 2, n_fs)
+
+    def send_out(kind):
+        a = (ro, ao)[kind]
+        dst, sem = out_block(kind, c, f)
+        remote(None, a, dst, sem, fs=beside, tp=owner)
+        remote(None, a, dst, sem, fs=across, tp=owner)
+        local(c == owner, a, dst, sem)
+        remote(c != owner, a, dst, sem, tp=peer)
+
+    def pass_out(kind):
+        cond, fsrc, to = ((c == owner, beside, across), (c != owner, across, beside))[kind]
+        for core in range(2):
+            block, sem = out_block(kind, core, fsrc)
+            pl.when(cond)(functools.partial(arrived, block, sem))
+            remote(cond, block, block, sem, fs=to)
+
+    send_out(0)
+
+    inputs[0].wait()
+    inputs[1].wait()
     x = tok[...].astype(F32)
     sq = x * x
     part = sq[:, :128]
@@ -385,30 +440,8 @@
                 remote(c == kind, block, block, wpsem.at[zs, f], slot=base[k - 1],
                        fs=lax.rem(f + k, n_fs))
 
-    fs_core = n_fs // 2
-    owner = f // fs_core
-    jf = lax.rem(f, fs_core)
-    out_rows, out_cols = ro.shape
-    for kind, a in enumerate((ro, ao)):
-        dst = wo.at[kind, pl.ds(pl.multiple_of(c * out_rows, out_rows), out_rows),
-                    pl.ds(pl.multiple_of(jf * out_cols, out_cols), out_cols)]
-        sem = osem.at[kind, c, jf]
-        for k in range(1, n_fs):
-            remote(None, a, dst, sem, fs=lax.rem(f + k, n_fs), tp=owner)
-        local(c == owner, a, dst, sem)
-        remote(c != owner, a, dst, sem, tp=peer)
-
-    for kind, cols in ((0, ret_cols), (1, att_cols)):
-        @pl.when(c == kind)
-        def _():
-            for n, (_, _, cd) in enumerate(pieces(0, kind)):
-                arrived(w.at[wrows(z * depth, depth), cd], wsem.at[z, n])
-            for i in range(1, n_sp):
-                zs = lax.rem(z + i, n_sp)
-                for k in range(1, n_fs):
-                    fs = lax.rem(f + k, n_fs)
-                    arrived(w.at[wrows(zs * depth + fs * quarter, quarter), pl.ds(0, cols)],
-                            wpsem.at[zs, fs])
+    send_out(1)
+
     for i in range(n_sp):
         arrived(sm.at[i], smsem.at[i])
     kv[pl.ds(0, WINDOW), :] = jnp.zeros((WINDOW, kv.shape[1]), BF16)
@@ -444,39 +477,6 @@
                 for s in range(1, heads_core):
                     got = jnp.where(sub == s, both_kv[:, n * kvw + s * HD : n * kvw + (s + 1) * HD], got)
                 kv[to, pl.ds(n * 128, HD)] = got.astype(BF16)
-
-    def peer_half(zs):
-        arrived(toks.at[zs, peer], tsem.at[zs, peer])
-
-    def later(zs, cond):
-        def run():
-            peer_half(zs)
-            project(zs)
-        if cond is None:
-            run()
-        else:
-            pl.when(cond)(run)
-
-    waiting = [(z, None)]
-    for d in range(1, n_sp):
-        new = []
-        for s in (-1, 1):
-            zs = z + s * d
-            ok = zs >= 0 if s < 0 else zs < n_sp
-            zs = jnp.clip(zs, 0, n_sp - 1)
-            pl.when(ok)(functools.partial(arrived, toks.at[zs, c], tsem.at[zs, c]))
-            if s < 0:
-                spread(zs, ok, z < n_sp - 1, None)
-            else:
-                spread(zs, ok, None, z > 0)
-            new.append((zs, ok))
-            if waiting:
-                later(*waiting.pop(0))
-        for item in waiting:
-            later(*item)
-        waiting = new
-    for item in waiting:
-        later(*item)
 
     lane = lax.broadcasted_iota(jnp.int32, (BLOCK, BLOCK), 1)
     row = lax.broadcasted_iota(jnp.int32, (BLOCK, BLOCK), 0)
@@ -504,8 +504,7 @@
     lane2 = lax.broadcasted_iota(jnp.int32, (WINDOW, 2 * WINDOW), 1)
     row2 = lax.broadcasted_iota(jnp.int32, (WINDOW, 2 * WINDOW), 0)
 
-    def attention(p, i):
-        b = p * per + i
+    def attention(b):
         at = pl.ds(pl.multiple_of(b * WINDOW, WINDOW), WINDOW)
         band = pl.ds(pl.multiple_of(b * WINDOW, WINDOW), 2 * WINDOW)
         k, v = kv[band, pl.ds(0, HD)], kv[band, pl.ds(128, HD)]
@@ -524,6 +523,77 @@
             res.append(dot((e / total).astype(BF16), v))
         hid[at, :] = jnp.concatenate(res, axis=1).astype(BF16)
 
+    def all_weights():
+        for kind, cols in ((0, ret_cols), (1, att_cols)):
+            @pl.when(c == kind)
+            def _():
+                for n, (_, _, cd) in enumerate(pieces(0, kind)):
+                    arrived(w.at[wrows(z * depth, depth), cd], wsem.at[z, n])
+                for i in range(1, n_sp):
+                    zs = lax.rem(z + i, n_sp)
+                    for k in range(1, n_fs):
+                        fs = lax.rem(f + k, n_fs)
+                        arrived(w.at[wrows(zs * depth + fs * quarter, quarter), pl.ds(0, cols)],
+                                wpsem.at[zs, fs])
+
+    def hand_on(p, cond):
+        block = hid.at[pl.ds(pl.multiple_of(p * rows, rows), rows)]
+        remote(both(cond, p != z), block, hin.at[c, z], hsem.at[c, z], sp=p)
+        local(both(cond, p == z), block, hin.at[c, z], hsem.at[c, z])
+
+    def land(d):
+        for s in (-1, 1):
+            zs = z + s * d
+            ok = zs >= 0 if s < 0 else zs < n_sp
+            zs = jnp.clip(zs, 0, n_sp - 1)
+            pl.when(ok)(functools.partial(arrived, toks.at[zs, c], tsem.at[zs, c]))
+            if s < 0:
+                spread(zs, ok, z < n_sp - 1, None)
+            else:
+                spread(zs, ok, None, z > 0)
+
+    def attend(first, last):
+        @pl.loop(first * per, last * per)
+        def _(b):
+            attention(b)
+
+    def take(d):
+        for s in (-1, 1) if d else (0,):
+            zs = z + s * d
+            ok = jnp.logical_and(zs >= 0, zs < n_sp)
+            zs = jnp.clip(zs, 0, n_sp - 1)
+
+            @pl.when(ok)
+            def _():
+                arrived(toks.at[zs, peer], tsem.at[zs, peer])
+                project(zs)
+
+            first = both(ok, both(is1, zs == 0))
+            if s > 0:
+                pl.when(both(ok, is1))(functools.partial(attend, zs, zs + 1))
+                hand_on(zs, both(ok, is1))
+            elif s < 0:
+                pl.when(both(ok, is1))(
+                    functools.partial(attend, zs + jnp.where(zs == 0, 0, 1), zs + 2)
+                )
+                hand_on(zs + 1, both(ok, is1))
+                hand_on(jnp.int32(0), first)
+            else:
+                pl.when(first)(functools.partial(attend, zs, zs + 1))
+                hand_on(jnp.int32(0), first)
+
+    for d in range(1, n_sp - 1):
+        land(d)
+    inputs[5].wait()
+    inputs[6].wait()
+    all_weights()
+    pass_out(0)
+    for d in range(n_sp - 1):
+        take(d)
+    land(n_sp - 1)
+    take(n_sp - 1)
+    pass_out(1)
+
     @pl.when(is0)
     def _():
         arrived(s0, ssem)
@@ -534,13 +604,7 @@
         def _():
             pl.loop(0, per)(functools.partial(retention, p))
 
-        @pl.when(is1)
-        def _():
-            pl.loop(0, per)(functools.partial(attention, p))
-
-        block = hid.at[pl.ds(p * rows, rows)]
-        remote(z != p, block, hin.at[c, z], hsem.at[c, z], sp=jnp.int32(p))
-        local(z == p, block, hin.at[c, z], hsem.at[c, z])
+        hand_on(jnp.int32(p), is0)
 
     for i in range(n_sp):
         zs = lax.rem(z + i, n_sp)
@@ -549,8 +613,11 @@
     for kind in range(2):
         for cs in range(2):
             for j in range(fs_core):
-                arrived(wo.at[kind, pl.ds(cs * out_rows, out_rows), pl.ds(j * out_cols, out_cols)],
-                        osem.at[kind, cs, j])
+                block, sem = out_block(kind, cs, jnp.int32(j))
+                passed = both(c == owner, beside == c * fs_core + j) if kind == 0 else both(
+                    c != owner, across == c * fs_core + j
+                )
+                pl.when(jnp.logical_not(passed))(functools.partial(arrived, block, sem))
     for zs in range(n_sp):
         arrived(hin.at[peer, zs], hsem.at[peer, zs])
 
@@ -580,20 +647,14 @@
     kv_heads = att_key.shape[1] // HD
     rows, half = tokens.shape[1:]
     whole_heads = (
-        n_tp == 2 and n_fs % 2 == 0 and heads * n_tp == n_sp and kv_heads == heads
+        n_tp == 2 and n_fs == 4 and heads * n_tp == n_sp and kv_heads == heads
         and att_query.shape[1] == ret_query.shape[1]
     )
     if not whole_heads:
         return shards(*args)
     depth = ret_query.shape[0]
     wide = heads * rows
-    decay = log_decay[0].reshape(1, wide)
-    small = jnp.concatenate([
-        jnp.pad(ret_gain[None], ((0, 0), (0, wide - ret_gain.shape[0]))),
-        decay,
-        jnp.zeros((SINK_ROW - 2, wide), F32),
-        jnp.broadcast_to(sink_logits[:, None], (sink_logits.shape[0], wide)),
-    ])
+    small = (SINK_ROW + sink_logits.shape[0], wide)
     h = DK // 2
     inverse = np.float32(1.0) / np.float32(10000.0) ** (np.arange(h, dtype=np.float32) / np.float32(h))
     angles = np.arange(n_sp * rows, dtype=np.float32)[:, None] * inverse[None, :]
@@ -606,15 +667,24 @@
     res = pl.pallas_call(
         functools.partial(fused, n_sp, n_fs),
         out_shape=jax.ShapeDtypeStruct((rows, half), BF16),
-        in_specs=[vm, vm] + [hbm] * 6 + [vm, hbm, hbm, hbm, vm, vm],
+        in_specs=[hbm] * 16,
         out_specs=vm,
         scratch_shapes=[
+            pltpu.VMEM((rows, half), BF16),
+            pltpu.VMEM((1, norm_gain.shape[0]), F32),
+            pltpu.VMEM(small, F32),
+            pltpu.VMEM((length, h), F32),
+            pltpu.VMEM((length, h), F32),
+            pltpu.VMEM((1, ret_gain.shape[0]), F32),
+            pltpu.VMEM((heads, rows), F32),
+            pltpu.VMEM((1, sink_logits.shape[0]), F32),
+            dma((7,)),
             pltpu.VMEM((n_sp, 2, rows, half), BF16),
             pltpu.VMEM((rows, 128), F32),
             pltpu.VMEM((rows, 128), F32),
             pltpu.VMEM((n_sp * depth, 3 * DK), BF16),
             pltpu.VMEM((2, 2 * ret_out.shape[0], n_fs // 2 * ret_out.shape[1]), BF16),
-            pltpu.VMEM((n_sp,) + small.shape, F32),
+            pltpu.VMEM((n_sp,) + small, F32),
             pltpu.VMEM((DK, DV), F32),
             pltpu.VMEM((length, 3 * DK), BF16),
             pltpu.VMEM((WINDOW + length, 256), BF16),
@@ -633,11 +703,11 @@
             dma,
         ],
         compiler_params=pltpu.CompilerParams(
-            collective_id=0, has_side_effects=True, vmem_limit_bytes=48 * 1024 * 1024
+            collective_id=0, has_side_effects=True, vmem_limit_bytes=67043328
         ),
     )(
         tokens[0], norm_gain[None], ret_query, ret_key, ret_value, att_query, att_key, att_value,
-        small, start_state[0], ret_out, att_out, cos, sin,
+        ret_gain[None], log_decay[0], sink_logits[None], start_state[0], ret_out, att_out, cos, sin,
     )
     return res[None]
 

time: 123 us -> 81.8 us (0.67)
  the two profiles are of different devices: /device:TPU:28 before, /device:TPU:25 now
where the time goes in v2:
time: 81.8 us; the launch traced here: 81.6 us
  Pallas kernels  79.7 us (97%)
  local copies, waits for them, and re-layouts  1.87 us (2%)
    pallas_call x1, Pallas kernels, layer(): pl.pallas_call(functools.partial(fused, n_sp, n_fs), out_shape=jax.ShapeD...  79.7 us
    unnamed x1, local copies, waits for them, and re-layouts  1.87 us

profile of v2, /device:TPU:25, one launch (start us, length us, event | category | flops | bytes accessed | tf_op | source)
XLA Modules:
  0.0 81.6 jit_solution(12010021182359788680)
XLA Ops:
  0.0 79.7 %shard_map.154 = bf16[256,1024]{1,0:T(8,128)(2,1)} custom-call(bf16[256,1024]{1,0:T(8,128)(2,1)} %bitcast.8, f32[1,2048]{1,0:T(1,128)} %bitcast.10, bf16[512,512]{1,0:T(8,128)(2,1)} %rq.1, bf16[512,512]{1,0:T(8,128)(2,1)} %rk.1, bf16[512,512]{1,0:T(8,128)(2,1)} %rv.1, bf16[512,512]{1,0:T(8,128)(2,1)} %aq.1, bf16[512,128]{1,0:T(8,128)(2,1)} %ak.1, ...), custom_call_target="tpu_custom_call" | custom-call | tf_op jit(solution)/shard_map/pallas_call | solution.py:667
  79.7 1.9 %copy.18 = bf16[1,256,1024]{2,1,0:T(8,128)(2,1)} copy(bf16[1,256,1024]{2,1,0:T(8,128)(2,1)} %bitcast.7) | data formatting | bytes 1048576

commit v3 on v2

--- a/solution.py
+++ b/solution.py
@@ -251,7 +251,7 @@
 def fused(
     n_sp, n_fs, tok_in, ngain_in, rq, rk, rv, aq, ak, av, gain_in, decay_in, sink_in, start, ro, ao, cos_in, sin_in, out,
     tok, ngain, small, cos, sin, gain_v, decay_v, sink_v, insem,
-    toks, ss_mine, ss_peer, w, wo, sm, s0, proj, kv, hid, hin, state,
+    toks, ss_mine, ss_peer, w, wo, sm, s0, proj, kv, hid, hin, state, total,
     send, wsem, wpsem, smsem, ssem, sssem, tsem, osem, hsem, lsem,
 ):
     z, f, c = lax.axis_index("sp"), lax.axis_index("fs"), lax.axis_index("tp")
@@ -348,8 +348,9 @@
         p = heads_core * c + j
         away = p != z
         here = p == z
+        decay = small.at[pl.ds(0, SINK_ROW)], sm.at[z, pl.ds(0, SINK_ROW)]
+        remote(away, *decay, smsem.at[z], sp=p, tp=jnp.int32(0))
         for kind in range(2):
-            remote(away, small, sm.at[z], smsem.at[z], sp=p, tp=jnp.int32(kind))
             for i, (a, cs, cd) in enumerate(pieces(j, kind)):
                 remote(
                     away, a.at[mine, cs], w.at[wrows(z * depth + f * quarter, quarter), cd],
@@ -395,6 +396,7 @@
             remote(cond, block, block, sem, fs=to)
 
     send_out(0)
+    send_out(1)
 
     inputs[0].wait()
     inputs[1].wait()
@@ -426,7 +428,7 @@
             act(c == kind, pl.ds(0, cols))
 
     for i in range(1, n_sp):
-        zs = lax.rem(z + i, n_sp)
+        zs = lax.rem(jnp.where(z < n_sp // 2, z + i, z + n_sp - i), n_sp)
         at = wrows(zs * depth + f * quarter, quarter)
         for kind in range(2):
             @pl.when(c == kind)
@@ -440,10 +442,6 @@
                 remote(c == kind, block, block, wpsem.at[zs, f], slot=base[k - 1],
                        fs=lax.rem(f + k, n_fs))
 
-    send_out(1)
-
-    for i in range(n_sp):
-        arrived(sm.at[i], smsem.at[i])
     kv[pl.ds(0, WINDOW), :] = jnp.zeros((WINDOW, kv.shape[1]), BF16)
 
     def project(zs):
@@ -541,16 +539,18 @@
         remote(both(cond, p != z), block, hin.at[c, z], hsem.at[c, z], sp=p)
         local(both(cond, p == z), block, hin.at[c, z], hsem.at[c, z])
 
+    near = jnp.where(z < n_sp // 2, -1, 1)
+
     def land(d):
-        for s in (-1, 1):
-            zs = z + s * d
-            ok = zs >= 0 if s < 0 else zs < n_sp
-            zs = jnp.clip(zs, 0, n_sp - 1)
-            pl.when(ok)(functools.partial(arrived, toks.at[zs, c], tsem.at[zs, c]))
-            if s < 0:
-                spread(zs, ok, z < n_sp - 1, None)
-            else:
-                spread(zs, ok, None, z > 0)
+        for s in (near, -near):
+            zs, to = z + s * d, z - s
+            ok = jnp.logical_and(zs >= 0, zs < n_sp)
+            onward = jnp.logical_and(ok, jnp.logical_and(to >= 0, to < n_sp))
+            zs, to = jnp.clip(zs, 0, n_sp - 1), jnp.clip(to, 0, n_sp - 1)
+            block = toks.at[zs, c]
+            pl.when(ok)(functools.partial(arrived, block, tsem.at[zs, c]))
+            remote(onward, block, block, tsem.at[zs, c], sp=to)
+            remote(ok, block, block, tsem.at[zs, c], tp=peer)
 
     def attend(first, last):
         @pl.loop(first * per, last * per)
@@ -584,15 +584,19 @@
 
     for d in range(1, n_sp - 1):
         land(d)
+    arrived(sm.at[z], smsem.at[z])
+    for i in range(1, n_sp):
+        zs = lax.rem(z + i, n_sp)
+        pl.when(is0)(functools.partial(arrived, sm.at[zs, pl.ds(0, SINK_ROW)], smsem.at[zs]))
     inputs[5].wait()
     inputs[6].wait()
     all_weights()
     pass_out(0)
+    pass_out(1)
     for d in range(n_sp - 1):
         take(d)
     land(n_sp - 1)
     take(n_sp - 1)
-    pass_out(1)
 
     @pl.when(is0)
     def _():
@@ -606,11 +610,13 @@
 
         hand_on(jnp.int32(p), is0)
 
-    for i in range(n_sp):
-        zs = lax.rem(z + i, n_sp)
-        arrived(hin.at[c, zs], hsem.at[c, zs])
-        remote(None, hin.at[c, zs], hin.at[c, zs], hsem.at[c, zs], tp=peer)
-    for kind in range(2):
+    width = hin.shape[3]
+    for kind in (1, 0):
+        for i in range(n_sp):
+            zs = lax.rem(z + i, n_sp)
+            block = hin.at[kind, zs]
+            arrived(block, hsem.at[kind, zs])
+            remote(c == kind, block, block, hsem.at[kind, zs], tp=peer)
         for cs in range(2):
             for j in range(fs_core):
                 block, sem = out_block(kind, cs, jnp.int32(j))
@@ -618,19 +624,18 @@
                     c != owner, across == c * fs_core + j
                 )
                 pl.when(jnp.logical_not(passed))(functools.partial(arrived, block, sem))
-    for zs in range(n_sp):
-        arrived(hin.at[peer, zs], hsem.at[peer, zs])
-
-    @pl.loop(0, out.shape[1] // 256)
-    def _(i):
-        cols = pl.ds(pl.multiple_of(i * 256, 256), 256)
-        acc = None
-        for kind in range(2):
+
+        @pl.loop(0, out.shape[1] // 256)
+        def _(i):
+            cols = pl.ds(pl.multiple_of(i * 256, 256), 256)
+            acc = total[:, cols] if kind == 0 else None
             for h in range(n_sp):
-                width = hin.shape[3]
                 term = dot(hin[kind, h], wo[kind, pl.ds(h * width, width), cols])
                 acc = term if acc is None else acc + term
-        out[:, cols] = acc.astype(BF16)
+            if kind == 0:
+                out[:, cols] = acc.astype(BF16)
+            else:
+                total[:, cols] = acc
 
     for cond, copy in sent:
         if cond is None:
@@ -691,6 +696,7 @@
             pltpu.VMEM((length, DV), BF16),
             pltpu.VMEM((2, n_sp, rows, DV), BF16),
             pltpu.VMEM((DK, DV), F32),
+            pltpu.VMEM((rows, half), F32),
             dma((100,)),
             dma((n_sp, 3)),
             dma((n_sp, n_fs)),

time: 81.8 us -> 80.7 us (0.987)
  the two profiles are of different devices: /device:TPU:25 before, /device:TPU:0 now
where the time goes in v3:
time: 80.7 us; the launch traced here: 79.2 us
  Pallas kernels  77.4 us (96%)
  local copies, waits for them, and re-layouts  1.87 us (2%)
    pallas_call x1, Pallas kernels, layer(): pl.pallas_call(functools.partial(fused, n_sp, n_fs), out_shape=jax.ShapeD...  77.4 us
    unnamed x1, local copies, waits for them, and re-layouts  1.87 us

profile of v3, /device:TPU:0, one launch (start us, length us, event | category | flops | bytes accessed | tf_op | source)
XLA Modules:
  0.0 79.2 jit_solution(4024429976778011525)
XLA Ops:
  0.0 77.4 %shard_map.154 = bf16[256,1024]{1,0:T(8,128)(2,1)} custom-call(bf16[256,1024]{1,0:T(8,128)(2,1)} %bitcast.8, f32[1,2048]{1,0:T(1,128)} %bitcast.10, bf16[512,512]{1,0:T(8,128)(2,1)} %rq.1, bf16[512,512]{1,0:T(8,128)(2,1)} %rk.1, bf16[512,512]{1,0:T(8,128)(2,1)} %rv.1, bf16[512,512]{1,0:T(8,128)(2,1)} %aq.1, bf16[512,128]{1,0:T(8,128)(2,1)} %ak.1, ...), custom_call_target="tpu_custom_call" | custom-call | tf_op jit(solution)/shard_map/pallas_call | solution.py:672
  77.4 1.9 %copy.18 = bf16[1,256,1024]{2,1,0:T(8,128)(2,1)} copy(bf16[1,256,1024]{2,1,0:T(8,128)(2,1)} %bitcast.7) | data formatting | bytes 1048576
